TPU v7x, 32 devices: a whole 2x2x4 slice. The times are simulated.
32 devices in a mesh: grp: 2 (over y), tp: 4 (over z), dp: 4 (over x, core).
Axes of the slice: x: 2, y: 2, z: 4, core: 2. Of those that a mesh axis runs over, the one named last changes fastest.
Arguments:
- tokens: bfloat16 [128, 4096], P('grp', 'dp'), parts along dimension 0, may hold values from -50 to 50
- lengths: int32 [128], P(('grp', 'dp')), parts along dimension 0, may hold values from 1 to 24, as said below
- norm_gain: float32 [2, 4096], P(None, 'dp'), may hold values from 0.1 to 1.9
- w_z: bfloat16 [2, 4096, 4096], P(None, 'dp', 'tp'), may hold values from -0.09375 to 0.09375
- w_x: bfloat16 [2, 4096, 4096], P(None, 'dp', 'tp'), may hold values from -0.09375 to 0.09375
- w_b: bfloat16 [2, 4096, 2048], P(None, 'dp', 'tp'), may hold values from -0.09375 to 0.09375
- w_c: bfloat16 [2, 4096, 2048], P(None, 'dp', 'tp'), may hold values from -0.09375 to 0.09375
- w_dt: bfloat16 [2, 4096, 64], P(None, 'dp'), may hold values from -0.09375 to 0.09375
- conv_weight: bfloat16 [2, 4, 8192], P(None, None, 'tp'), may hold values from -3 to 3
- dt_bias: float32 [2, 64], P(None, 'tp'), may hold values from -6 to -1.5
- a_log: float32 [2, 64], P(None, 'tp'), may hold values from 0 to 2.77
- d_skip: float32 [2, 64], P(None, 'tp'), may hold values from 0.1 to 1.9
- out_gain: float32 [2, 4096], P(None, 'tp'), may hold values from 0.1 to 1.9
- w_out: bfloat16 [2, 4096, 4096], P(None, 'tp', 'dp'), may hold values from -0.09375 to 0.09375
- conv_state: bfloat16 [2, 128, 3, 8192], P(None, ('grp', 'dp'), None, 'tp'), parts along dimension 1, may hold values from -6 to 6
- ssm_state: float32 [2, 128, 64, 64, 128], P(None, ('grp', 'dp'), 'tp'), parts along dimension 1, may hold values from -2 to 2
Outputs:
- mixed_out: bfloat16 [128, 4096], P('grp', 'dp'), parts along dimension 0
- conv_new: bfloat16 [2, 128, 3, 8192], P(None, ('grp', 'dp'), None, 'tp'), parts along dimension 1
- ssm_new: float32 [2, 128, 64, 64, 128], P(None, ('grp', 'dp'), 'tp'), parts along dimension 1
There are 2 independent parts, one for each index of `grp`. A program takes and returns all parts, laid end to end along the dimension named above; an argument that names none is the same for every part. Nothing has to cross between parts.
Inputs may be any that keep to these rules, and one draw needn't show every extreme that they name: `lengths`: each part has at least one sequence of length 24.
All inputs are finite; a program needn't handle non-finite values.
Results may differ from a plain program's by a relative error of at most 0.012.
Values may be sent and summed in bfloat16 or wider, within the bound.
A program may use at most 128 MiB of HBM per device.

v0:
```python
import functools

import jax
import jax.numpy as jnp
from jax import lax
from jax.experimental import pallas as pl
from jax.experimental.pallas import tpu as pltpu
from jax.sharding import PartitionSpec as P

D = 4096
HEADS = 64
GROUPS = 16
HEAD_DIM = 64
STATE = 128
CONV_W = 4
PER_GROUP = HEADS // GROUPS
WIDTH_X = PER_GROUP * HEAD_DIM
GROUP_W = WIDTH_X + 2 * STATE
EPSILON = 1e-06
MESH = pl.DeviceIdType.MESH
BF16 = jnp.bfloat16
F32 = jnp.float32


def silu(t):
    return t / (1.0 + jnp.exp(-t))


def block_kernel(
    nd, nt,
    tokens_ref, lens_ref, gain_ref, bias_ref, alog_ref, skip_ref, ogain_ref, taps_ref, conv_ref,
    wz_hbm, wx_hbm, wb_hbm, wc_hbm, wdt_hbm, wo_hbm, state_hbm,
    out_ref, cur_ref, kept_ref, dec_ref, sx_ref, wk_ref,
    wz, wx, wb, wc, wdt, wo, state,
    snd_e, snd_x, snd_b, snd_c, snd_z,
    rcv_e, rcv_x, rcv_b, rcv_c, rcv_z,
    mixes, snd_o, rcv_o, stream, normed_s, rk_s, y_s,
    w_sem, st_sem, dps, dpr, ags, agr, rss, rsr, tgs, tgr,
):
    dp = lax.axis_index("dp")
    tp = lax.axis_index("tp")
    layers = gain_ref.shape[0]
    seqs = lens_ref.shape[1]
    batch = nd * seqs
    rows = batch // nt
    dloc = gain_ref.shape[1]
    width = wx.shape[2]
    lgroups = width // WIDTH_X

    pairs = ((wdt_hbm, wdt), (wx_hbm, wx), (wb_hbm, wb), (wc_hbm, wc), (wz_hbm, wz), (wo_hbm, wo))

    def weight(layer, at):
        src, dst = pairs[at]
        return pltpu.make_async_copy(src.at[layer], dst.at[layer], w_sem.at[layer, at])

    def states(layer):
        return pltpu.make_async_copy(state_hbm.at[layer], state.at[layer], st_sem.at[layer])

    for at in range(5):
        weight(0, at).start()

    barrier = pltpu.get_barrier_semaphore()
    for k in range(1, nd):
        pl.semaphore_signal(
            barrier, inc=1, device_id={"dp": lax.rem(dp + k, nd)}, device_id_type=MESH
        )
    for k in range(1, nt):
        pl.semaphore_signal(
            barrier, inc=1, device_id={"tp": lax.rem(tp + k, nt)}, device_id_type=MESH
        )
    pl.semaphore_wait(barrier, nd - 1 + nt - 1)

    def scatter(layer, snd, rcv, at):
        copies = []
        for k in range(1, nd):
            peer = lax.rem(dp + k, nd)
            copy = pltpu.make_async_remote_copy(
                src_ref=snd.at[layer, peer],
                dst_ref=rcv.at[layer, k - 1],
                send_sem=dps.at[layer, at, k - 1],
                recv_sem=dpr.at[layer, at, k - 1],
                device_id={"dp": peer},
                device_id_type=MESH,
            )
            copy.start()
            copies.append(copy)
        return copies

    def gathered(copies, layer, snd, rcv):
        for copy in copies:
            copy.wait_recv()
        total = snd[layer, dp].astype(F32)
        for k in range(nd - 1):
            total = total + rcv[layer, k].astype(F32)
        return total

    heads_all = wdt.shape[1]
    lheads = bias_ref.shape[1]

    def expand(values, offset):
        count = values.shape[1]
        head = lax.broadcasted_iota(jnp.int32, (count, width), 0)
        lane = lax.broadcasted_iota(jnp.int32, (count, width), 1)
        pick = jnp.where(head == lane // HEAD_DIM + offset, 1.0, 0.0).astype(F32)
        return jnp.dot(
            values, pick, preferred_element_type=F32, precision=lax.Precision.HIGHEST
        )

    bias = expand(bias_ref[...], 0)
    rate = jnp.exp(expand(alog_ref[...], 0))
    skip = expand(skip_ref[...], 0)
    spread = jnp.broadcast_to(lens_ref[...].astype(F32), (seqs, seqs))
    diagonal = lax.broadcasted_iota(jnp.int32, (seqs, seqs), 0) == lax.broadcasted_iota(
        jnp.int32, (seqs, seqs), 1
    )
    lens = jnp.sum(jnp.where(diagonal, spread, 0.0), axis=1, keepdims=True)
    pending = []

    for layer in range(layers):
        source = tokens_ref if layer == 0 else stream.at[layer - 1]
        wide = source[...].astype(F32).reshape(batch, dloc)
        squares = jnp.sum(wide * wide, axis=-1, keepdims=True)
        normed_s[...] = (wide * gain_ref[layer : layer + 1, :]).astype(BF16)

        def project(w_ref, snd, layer=layer):
            n = w_ref.shape[2]
            tile = min(n, 256)

            def step(j, carry):
                cols = pl.ds(pl.multiple_of(j * tile, tile), tile)
                part = jnp.dot(
                    normed_s[...], w_ref[layer, :, cols], preferred_element_type=F32
                )
                snd[layer, :, :, cols] = part.reshape(nd, seqs, tile).astype(snd.dtype)
                return carry

            lax.fori_loop(0, n // tile, step, 0)

        weight(layer, 0).wait()
        part_dt = lax.dot_general(
            normed_s[...], wdt[layer], (((1,), (1,)), ((), ())), preferred_element_type=F32
        )
        snd_e[layer, :, :, 0:128] = jnp.zeros((nd, seqs, 128), F32)
        snd_e[layer, :, :, 0:heads_all] = part_dt.reshape(nd, seqs, heads_all)
        snd_e[layer, :, :, 128:256] = jnp.broadcast_to(squares, (batch, 128)).reshape(
            nd, seqs, 128
        )
        weight(layer, 1).wait()
        project(wx, snd_x)
        copies_x = scatter(layer, snd_x, rcv_x, 1)
        copies_e = scatter(layer, snd_e, rcv_e, 0)
        weight(layer, 2).wait()
        project(wb, snd_b)
        copies_b = scatter(layer, snd_b, rcv_b, 2)
        weight(layer, 3).wait()
        project(wc, snd_c)
        copies_c = scatter(layer, snd_c, rcv_c, 3)
        weight(layer, 4).wait()
        if layer == 0:
            states(0).start()
            weight(0, 5).start()
        project(wz, snd_z)
        copies_z = scatter(layer, snd_z, rcv_z, 4)
        if layer + 1 < layers:
            for at in range(6):
                weight(layer + 1, at).start()
            states(layer + 1).start()

        extra = gathered(copies_e, layer, snd_e, rcv_e)
        inverse = lax.rsqrt(extra[:, 128:129] / D + EPSILON)
        raw = expand(extra[:, 0:heads_all] * inverse, tp * lheads)
        softin = raw + bias[layer : layer + 1, :]
        step = jnp.maximum(softin, 0.0) + jnp.log1p(jnp.exp(-jnp.abs(softin)))
        decay = jnp.exp(-rate[layer : layer + 1, :] * step)
        decay = jnp.where(lens >= 2, decay, 0.0)

        values = (gathered(copies_x, layer, snd_x, rcv_x) * inverse).astype(BF16)
        writes = (gathered(copies_b, layer, snd_b, rcv_b) * inverse).astype(BF16)
        reads = (gathered(copies_c, layer, snd_c, rcv_c) * inverse).astype(BF16)
        pieces = []
        for g in range(lgroups):
            pieces.append(values[:, g * WIDTH_X : (g + 1) * WIDTH_X])
            pieces.append(writes[:, g * STATE : (g + 1) * STATE])
            pieces.append(reads[:, g * STATE : (g + 1) * STATE])
        current = jnp.concatenate(pieces, axis=1)
        cur_ref[layer] = current
        summed = current.astype(F32) * taps_ref[
            layer, CONV_W - 1 : CONV_W, :
        ].astype(F32)
        for tap in range(CONV_W - 1):
            past = conv_ref[layer, tap].astype(F32)
            past = jnp.where(lens >= CONV_W - tap, past, 0.0)
            if tap >= 1:
                kept_ref[layer, tap - 1] = past.astype(BF16)
            summed = summed + past * taps_ref[layer, tap : tap + 1, :].astype(F32)
        active = silu(summed)
        head_in = jnp.concatenate(
            [active[:, g * GROUP_W : g * GROUP_W + WIDTH_X] for g in range(lgroups)], axis=1
        )
        wk = [
            active[:, g * GROUP_W + WIDTH_X : g * GROUP_W + WIDTH_X + STATE]
            for g in range(lgroups)
        ]
        rk = [active[:, g * GROUP_W + WIDTH_X + STATE : (g + 1) * GROUP_W] for g in range(lgroups)]
        stepx = step * head_in
        dec_ref[layer] = decay
        sx_ref[layer] = stepx
        wk_ref[layer] = jnp.concatenate(wk, axis=1)
        rk_s[...] = jnp.concatenate(rk, axis=1)

        states(layer).wait()

        def read_eight(b, carry, layer=layer):
            at = pl.ds(pl.multiple_of(b * 8, 8), 8)
            keys = rk_s[at, :]
            lines = []
            for i in range(8):
                outs = []
                for g in range(lgroups):
                    row = keys[i : i + 1, g * STATE : (g + 1) * STATE]
                    lhs = jnp.broadcast_to(row, (16, STATE)).astype(BF16)
                    held = state[layer, b * 8 + i, g * PER_GROUP : (g + 1) * PER_GROUP]
                    held = held.reshape(WIDTH_X, STATE).astype(BF16)
                    res = lax.dot_general(
                        lhs, held, (((1,), (1,)), ((), ())), preferred_element_type=F32
                    )
                    outs.append(res[0:1])
                lines.append(jnp.concatenate(outs, axis=1))
            y_s[at, :] = jnp.concatenate(lines, axis=0)
            return carry

        lax.fori_loop(0, seqs // 8, read_eight, 0)
        readout = decay * y_s[...] + skip[layer : layer + 1, :] * head_in
        gate = (gathered(copies_z, layer, snd_z, rcv_z) * inverse).astype(BF16).astype(F32)
        gate = silu(gate)
        mixed = []
        for g in range(lgroups):
            cols = slice(g * WIDTH_X, (g + 1) * WIDTH_X)
            cross = jnp.sum(wk[g] * rk[g], axis=-1, keepdims=True)
            gated = (readout[:, cols] + stepx[:, cols] * cross) * gate[:, cols]
            norm = lax.rsqrt(jnp.mean(gated * gated, axis=-1, keepdims=True) + EPSILON)
            mixed.append(gated * norm * ogain_ref[layer : layer + 1, cols])
        mixes[layer, dp] = jnp.concatenate(mixed, axis=1).astype(BF16)
        copies_m = []
        for k in range(1, nd):
            copy = pltpu.make_async_remote_copy(
                src_ref=mixes.at[layer, dp],
                dst_ref=mixes.at[layer, dp],
                send_sem=ags.at[layer, k - 1],
                recv_sem=agr.at[layer, k - 1],
                device_id={"dp": lax.rem(dp + k, nd)},
                device_id_type=MESH,
            )
            copy.start()
            copies_m.append(copy)
        weight(layer, 5).wait()
        for copy in copies_m:
            copy.wait_recv()

        tile = min(dloc, 256)

        def project_out(j, carry, layer=layer):
            cols = pl.ds(pl.multiple_of(j * tile, tile), tile)
            lhs = mixes[layer].reshape(batch, width)
            part = jnp.dot(lhs, wo[layer, :, cols], preferred_element_type=F32)
            snd_o[layer, :, :, cols] = part.reshape(nt, rows, tile).astype(BF16)
            return carry

        lax.fori_loop(0, dloc // tile, project_out, 0)
        copies_o = []
        for k in range(1, nt):
            peer = lax.rem(tp + k, nt)
            copy = pltpu.make_async_remote_copy(
                src_ref=snd_o.at[layer, peer],
                dst_ref=rcv_o.at[layer, k - 1],
                send_sem=rss.at[layer, k - 1],
                recv_sem=rsr.at[layer, k - 1],
                device_id={"tp": peer},
                device_id_type=MESH,
            )
            copy.start()
            copies_o.append(copy)
        total = source[tp].astype(F32) + snd_o[layer, tp].astype(F32)
        for k in range(nt - 1):
            copies_o[k].wait_recv()
            total = total + rcv_o[layer, k].astype(F32)
        stream[layer, tp] = total.astype(BF16)
        copies_s = []
        for k in range(1, nt):
            copy = pltpu.make_async_remote_copy(
                src_ref=stream.at[layer, tp],
                dst_ref=stream.at[layer, tp],
                send_sem=tgs.at[layer, k - 1],
                recv_sem=tgr.at[layer, k - 1],
                device_id={"tp": lax.rem(tp + k, nt)},
                device_id_type=MESH,
            )
            copy.start()
            copies_s.append(copy)
        for copy in copies_s:
            copy.wait_recv()
        for group in (copies_e, copies_x, copies_b, copies_c, copies_z, copies_m, copies_o, copies_s):
            pending.extend(group)

    out_ref[...] = stream[layers - 1]
    for copy in pending:
        copy.wait_send()


def state_kernel(
    stream_ref, cur_ref, kept_ref, dec_ref, sx_ref, wk_ref, state_ref, out_ref, conv_ref, new_ref
):
    @pl.when(jnp.logical_and(pl.program_id(0) == 0, pl.program_id(1) == 0))
    def small():
        out_ref[...] = stream_ref[...]
        conv_ref[:, 0 : CONV_W - 2] = kept_ref[...]
        conv_ref[:, CONV_W - 2] = cur_ref[...]

    count = state_ref.shape[1]
    first = pl.program_id(1) * count
    width = dec_ref.shape[2]
    at = pl.ds(pl.multiple_of(first // 8 * 8, 8), 8)
    layer = pl.program_id(0)
    place = lax.rem(first, 8)

    def rows_of(ref):
        block = ref[layer, at, :]
        rows = block[0:count]
        for j in range(count, 8, count):
            rows = jnp.where(place == j, block[j : j + count], rows)
        return rows

    decs, sxs, wks = rows_of(dec_ref), rows_of(sx_ref), rows_of(wk_ref)
    for i in range(count):
        dec = jnp.broadcast_to(decs[i : i + 1], (64, width))
        sx = jnp.broadcast_to(sxs[i : i + 1], (64, width))
        cols = jnp.concatenate([dec, sx], axis=0).T
        for g in range(width // WIDTH_X):
            part = cols[g * WIDTH_X : (g + 1) * WIDTH_X]
            held = state_ref[0, i, g * PER_GROUP : (g + 1) * PER_GROUP].reshape(WIDTH_X, STATE)
            write = wks[i : i + 1, g * STATE : (g + 1) * STATE]
            new = part[:, 0:1] * held + part[:, 64:65] * write
            new_ref[0, i, g * PER_GROUP : (g + 1) * PER_GROUP] = new.reshape(
                PER_GROUP, HEAD_DIM, STATE
            )


def body(
    nd, nt,
    tokens, lengths, norm_gain, w_z, w_x, w_b, w_c, w_dt, conv_weight,
    dt_bias, a_log, d_skip, out_gain, w_out, conv_state, ssm_state,
):
    layers = w_z.shape[0]
    batch, dloc = tokens.shape
    seqs = lengths.shape[0]
    rows = batch // nt
    width = w_x.shape[2]
    keys = w_b.shape[2]
    turned = jnp.swapaxes(w_dt, 1, 2)
    conv_w = conv_weight.shape[2]
    vmem = pl.BlockSpec(memory_space=pltpu.VMEM)
    anywhere = pl.BlockSpec(memory_space=pl.ANY)
    dma = pltpu.SemaphoreType.DMA
    sizes = (width, keys, keys, width)
    stream, current, kept, dec, sx, wk = pl.pallas_call(
        functools.partial(block_kernel, nd, nt),
        out_shape=(
            jax.ShapeDtypeStruct((nt, rows, dloc), BF16),
            jax.ShapeDtypeStruct((layers, seqs, conv_w), BF16),
            jax.ShapeDtypeStruct((layers, CONV_W - 2, seqs, conv_w), BF16),
            jax.ShapeDtypeStruct((layers, seqs, width), F32),
            jax.ShapeDtypeStruct((layers, seqs, width), F32),
            jax.ShapeDtypeStruct((layers, seqs, keys), F32),
        ),
        in_specs=[vmem] * 9 + [anywhere] * 7,
        out_specs=[vmem] * 6,
        scratch_shapes=[
            pltpu.VMEM(w_z.shape, BF16),
            pltpu.VMEM(w_x.shape, BF16),
            pltpu.VMEM(w_b.shape, BF16),
            pltpu.VMEM(w_c.shape, BF16),
            pltpu.VMEM(turned.shape, BF16),
            pltpu.VMEM(w_out.shape, BF16),
            pltpu.VMEM(ssm_state.shape, F32),
            pltpu.VMEM((layers, nd, seqs, 256), F32),
            *[pltpu.VMEM((layers, nd, seqs, n), BF16) for n in sizes],
            pltpu.VMEM((layers, nd - 1, seqs, 256), F32),
            *[pltpu.VMEM((layers, nd - 1, seqs, n), BF16) for n in sizes],
            pltpu.VMEM((layers, nd, seqs, width), BF16),
            pltpu.VMEM((layers, nt, rows, dloc), BF16),
            pltpu.VMEM((layers, nt - 1, rows, dloc), BF16),
            pltpu.VMEM((layers, nt, rows, dloc), BF16),
            pltpu.VMEM((batch, dloc), BF16),
            pltpu.VMEM((seqs, keys), F32),
            pltpu.VMEM((seqs, width), F32),
            dma((layers, 6)),
            dma((layers,)),
            dma((layers, 5, nd - 1)),
            dma((layers, 5, nd - 1)),
            dma((layers, nd - 1)),
            dma((layers, nd - 1)),
            dma((layers, nt - 1)),
            dma((layers, nt - 1)),
            dma((layers, nt - 1)),
            dma((layers, nt - 1)),
        ],
        compiler_params=pltpu.CompilerParams(
            collective_id=0, has_side_effects=True, vmem_limit_bytes=56 * 1024 * 1024
        ),
    )(
        tokens.reshape(nt, rows, dloc), lengths[None, :], norm_gain, dt_bias, a_log, d_skip,
        out_gain, conv_weight, jnp.transpose(conv_state, (0, 2, 1, 3)),
        w_z, w_x, w_b, w_c, turned, w_out, ssm_state,
    )
    step = 2
    block = (1, step) + ssm_state.shape[2:]
    mixed_out, conv_new, ssm_new = pl.pallas_call(
        state_kernel,
        grid=(layers, seqs // step),
        out_shape=(
            jax.ShapeDtypeStruct(stream.shape, BF16),
            jax.ShapeDtypeStruct((layers, CONV_W - 1, seqs, conv_w), BF16),
            jax.ShapeDtypeStruct(ssm_state.shape, F32),
        ),
        in_specs=[vmem] * 6 + [pl.BlockSpec(block, lambda l, s: (l, s, 0, 0, 0))],
        out_specs=(vmem, vmem, pl.BlockSpec(block, lambda l, s: (l, s, 0, 0, 0))),
    )(stream, current, kept, dec, sx, wk, ssm_state)
    return mixed_out.reshape(batch, dloc), jnp.transpose(conv_new, (0, 2, 1, 3)), ssm_new


def solution(mesh):
    placed = (
        P("grp", "dp"),
        P(("grp", "dp")),
        P(None, "dp"),
        P(None, "dp", "tp"),
        P(None, "dp", "tp"),
        P(None, "dp", "tp"),
        P(None, "dp", "tp"),
        P(None, "dp", None),
        P(None, None, "tp"),
        P(None, "tp"),
        P(None, "tp"),
        P(None, "tp"),
        P(None, "tp"),
        P(None, "tp", "dp"),
        P(None, ("grp", "dp"), None, "tp"),
        P(None, ("grp", "dp"), "tp", None, None),
    )
    return jax.shard_map(
        functools.partial(body, mesh.shape["dp"], mesh.shape["tp"]),
        mesh=mesh,
        in_specs=placed,
        out_specs=(
            P("grp", "dp"),
            P(None, ("grp", "dp"), None, "tp"),
            P(None, ("grp", "dp"), "tp", None, None),
        ),
        check_vma=False,
    )
```

profile of v0, /device:TPU:0, one launch (start us, length us, event | category | flops | bytes accessed | tf_op | source)
XLA Modules:
  0.0 73.1 jit_solution(9126497184654725461)
XLA Ops:
  0.6 49.7 %shard_map.175 = (bf16[4,16,1024]{2,1,0:T(8,128)(2,1)}, bf16[2,16,2048]{2,1,0:T(8,128)(2,1)}, bf16[2,2,16,2048]{3,2,1,0:T(8,128)(2,1)}, f32[2,16,1024]{2,1,0:T(8...) custom-call(bf16[4,16,1024]{2,1,0:T(8,128)(2,1)} %bitcast.8, s32[1,16]{1,0:T(1,128)} %bitcast.9, ...), custom_call_target="tpu_custom_call" | custom-call | tf_op jit(solution)/shard_map/pallas_call | solution.py:365
  50.3 22.7 %shard_map.176 = (bf16[4,16,1024]{2,1,0:T(8,128)(2,1)}, bf16[2,3,16,2048]{3,2,1,0:T(8,128)(2,1)}, f32[2,16,16,64,128]{4,3,2,1,0:T(8,128)}) custom-call(bf16[4,16,1024]{2,1,0:T(8,128)(2,1)} %get-tuple-element.12.stream_ref, bf16[2,16,2048]{2,1,0:T(8,128)(2,1)} %get-tuple-element.13.cur_ref, bf16[2,2,16,2048]{3,2,1,0:T(8,128)(2,1)} %get-tuple-element.14.kept_ref, ...), custom_call_target="tpu_custom_call" | custom-call | tf_op jit(solution)/shard_map/pallas_call | solution.py:417
where the time goes:
time: 73.7 us; the launch traced here: 73.1 us
  Pallas kernels  72.4 us (98%)
    pallas_call x1, Pallas kernels, body(): pl.pallas_call(functools.partial(block_kernel, nd, nt), out_shape=(jax.Sh...  49.7 us
    pallas_call x1, Pallas kernels, body(): pl.pallas_call(state_kernel, grid=(layers, seqs // step), out_shape=(jax....  22.7 us

commit v1 on v0

--- a/solution.py
+++ b/solution.py
@@ -22,20 +22,33 @@
 F32 = jnp.float32
 
 
+SCOPE = []
+
+
+def mark(name):
+    if SCOPE:
+        SCOPE.pop().__exit__(None, None, None)
+    if name:
+        scope = jax.named_scope("m:" + name)
+        scope.__enter__()
+        SCOPE.append(scope)
+
+
 def silu(t):
     return t / (1.0 + jnp.exp(-t))
 
 
 def block_kernel(
     nd, nt,
+    tokens_hbm, lens_hbm, gain_hbm, bias_hbm, alog_hbm, skip_hbm, ogain_hbm, taps_hbm, conv_hbm,
+    wz_hbm, wx_hbm, wb_hbm, wc_hbm, wdt_hbm, wo_hbm, state_hbm,
+    out_ref, kept_ref, state,
     tokens_ref, lens_ref, gain_ref, bias_ref, alog_ref, skip_ref, ogain_ref, taps_ref, conv_ref,
-    wz_hbm, wx_hbm, wb_hbm, wc_hbm, wdt_hbm, wo_hbm, state_hbm,
-    out_ref, cur_ref, kept_ref, dec_ref, sx_ref, wk_ref,
-    wz, wx, wb, wc, wdt, wo, state,
+    wz, wx, wb, wc, wdt, wo,
     snd_e, snd_x, snd_b, snd_c, snd_z,
     rcv_e, rcv_x, rcv_b, rcv_c, rcv_z,
-    mixes, snd_o, rcv_o, stream, normed_s, rk_s, y_s,
-    w_sem, st_sem, dps, dpr, ags, agr, rss, rsr, tgs, tgr,
+    mixes, snd_o, rcv_o, stream, normed_s, rk_s, y_s, wk_s, cols_s,
+    w_sem, st_sem, in_sem, dps, dpr, ags, agr, rss, rsr, tgs, tgr,
 ):
     dp = lax.axis_index("dp")
     tp = lax.axis_index("tp")
@@ -56,9 +69,22 @@
     def states(layer):
         return pltpu.make_async_copy(state_hbm.at[layer], state.at[layer], st_sem.at[layer])
 
+    mark("start")
+    arrivals = [
+        pltpu.make_async_copy(src, dst, in_sem.at[i])
+        for i, (src, dst) in enumerate((
+            (tokens_hbm, tokens_ref), (gain_hbm, gain_ref), (lens_hbm, lens_ref),
+            (bias_hbm, bias_ref), (alog_hbm, alog_ref), (skip_hbm, skip_ref),
+            (ogain_hbm, ogain_ref), (taps_hbm, taps_ref), (conv_hbm, conv_ref),
+        ))
+    ]
+    for copy in arrivals[:8]:
+        copy.start()
     for at in range(5):
         weight(0, at).start()
-
+    arrivals[8].start()
+
+    mark("barrier")
     barrier = pltpu.get_barrier_semaphore()
     for k in range(1, nd):
         pl.semaphore_signal(
@@ -94,6 +120,9 @@
             total = total + rcv[layer, k].astype(F32)
         return total
 
+    mark("prep")
+    for copy in arrivals[:8]:
+        copy.wait()
     heads_all = wdt.shape[1]
     lheads = bias_ref.shape[1]
 
@@ -117,6 +146,7 @@
     pending = []
 
     for layer in range(layers):
+        mark("norm")
         source = tokens_ref if layer == 0 else stream.at[layer - 1]
         wide = source[...].astype(F32).reshape(batch, dloc)
         squares = jnp.sum(wide * wide, axis=-1, keepdims=True)
@@ -124,7 +154,7 @@
 
         def project(w_ref, snd, layer=layer):
             n = w_ref.shape[2]
-            tile = min(n, 256)
+            tile = min(n, 1024)
 
             def step(j, carry):
                 cols = pl.ds(pl.multiple_of(j * tile, tile), tile)
@@ -136,25 +166,28 @@
 
             lax.fori_loop(0, n // tile, step, 0)
 
+        mark("proj_dt")
         weight(layer, 0).wait()
         part_dt = lax.dot_general(
             normed_s[...], wdt[layer], (((1,), (1,)), ((), ())), preferred_element_type=F32
         )
-        snd_e[layer, :, :, 0:128] = jnp.zeros((nd, seqs, 128), F32)
-        snd_e[layer, :, :, 0:heads_all] = part_dt.reshape(nd, seqs, heads_all)
-        snd_e[layer, :, :, 128:256] = jnp.broadcast_to(squares, (batch, 128)).reshape(
-            nd, seqs, 128
-        )
+        snd_e[layer] = jnp.concatenate(
+            [part_dt, jnp.broadcast_to(squares, (batch, heads_all))], axis=1
+        ).reshape(nd, seqs, 2 * heads_all)
+        mark("proj_x")
         weight(layer, 1).wait()
         project(wx, snd_x)
         copies_x = scatter(layer, snd_x, rcv_x, 1)
         copies_e = scatter(layer, snd_e, rcv_e, 0)
+        mark("proj_b")
         weight(layer, 2).wait()
         project(wb, snd_b)
         copies_b = scatter(layer, snd_b, rcv_b, 2)
+        mark("proj_c")
         weight(layer, 3).wait()
         project(wc, snd_c)
         copies_c = scatter(layer, snd_c, rcv_c, 3)
+        mark("proj_z")
         weight(layer, 4).wait()
         if layer == 0:
             states(0).start()
@@ -166,24 +199,29 @@
                 weight(layer + 1, at).start()
             states(layer + 1).start()
 
+        mark("wait_e")
         extra = gathered(copies_e, layer, snd_e, rcv_e)
-        inverse = lax.rsqrt(extra[:, 128:129] / D + EPSILON)
+        inverse = lax.rsqrt(extra[:, heads_all : heads_all + 1] / D + EPSILON)
         raw = expand(extra[:, 0:heads_all] * inverse, tp * lheads)
         softin = raw + bias[layer : layer + 1, :]
         step = jnp.maximum(softin, 0.0) + jnp.log1p(jnp.exp(-jnp.abs(softin)))
         decay = jnp.exp(-rate[layer : layer + 1, :] * step)
         decay = jnp.where(lens >= 2, decay, 0.0)
 
+        mark("wait_xbc")
         values = (gathered(copies_x, layer, snd_x, rcv_x) * inverse).astype(BF16)
         writes = (gathered(copies_b, layer, snd_b, rcv_b) * inverse).astype(BF16)
         reads = (gathered(copies_c, layer, snd_c, rcv_c) * inverse).astype(BF16)
+        mark("conv")
+        if layer == 0:
+            arrivals[8].wait()
         pieces = []
         for g in range(lgroups):
             pieces.append(values[:, g * WIDTH_X : (g + 1) * WIDTH_X])
             pieces.append(writes[:, g * STATE : (g + 1) * STATE])
             pieces.append(reads[:, g * STATE : (g + 1) * STATE])
         current = jnp.concatenate(pieces, axis=1)
-        cur_ref[layer] = current
+        kept_ref[layer, CONV_W - 2] = current
         summed = current.astype(F32) * taps_ref[
             layer, CONV_W - 1 : CONV_W, :
         ].astype(F32)
@@ -203,13 +241,14 @@
         ]
         rk = [active[:, g * GROUP_W + WIDTH_X + STATE : (g + 1) * GROUP_W] for g in range(lgroups)]
         stepx = step * head_in
-        dec_ref[layer] = decay
-        sx_ref[layer] = stepx
-        wk_ref[layer] = jnp.concatenate(wk, axis=1)
+        for g in range(lgroups):
+            wk_s[g] = wk[g]
         rk_s[...] = jnp.concatenate(rk, axis=1)
 
+        mark("wait_state")
         states(layer).wait()
 
+        mark("readout")
         def read_eight(b, carry, layer=layer):
             at = pl.ds(pl.multiple_of(b * 8, 8), 8)
             keys = rk_s[at, :]
@@ -230,6 +269,7 @@
             return carry
 
         lax.fori_loop(0, seqs // 8, read_eight, 0)
+        mark("wait_z_gate")
         readout = decay * y_s[...] + skip[layer : layer + 1, :] * head_in
         gate = (gathered(copies_z, layer, snd_z, rcv_z) * inverse).astype(BF16).astype(F32)
         gate = silu(gate)
@@ -241,6 +281,7 @@
             norm = lax.rsqrt(jnp.mean(gated * gated, axis=-1, keepdims=True) + EPSILON)
             mixed.append(gated * norm * ogain_ref[layer : layer + 1, cols])
         mixes[layer, dp] = jnp.concatenate(mixed, axis=1).astype(BF16)
+        mark("send_m")
         copies_m = []
         for k in range(1, nd):
             copy = pltpu.make_async_remote_copy(
@@ -253,11 +294,32 @@
             )
             copy.start()
             copies_m.append(copy)
+        mark("update")
+        cols_s[...] = jnp.concatenate(
+            [stepx, decay, jnp.zeros((128 - 2 * seqs, width), F32)], axis=0
+        ).T
+
+        def update(h, carry, layer=layer):
+            first = pl.multiple_of(h * HEAD_DIM, HEAD_DIM)
+            adds = cols_s[pl.ds(first, HEAD_DIM), :]
+            keeps = cols_s[pl.ds(first, 8), :]
+            keys = wk_s[h // PER_GROUP]
+            for i in range(seqs):
+                keep = jnp.broadcast_to(keeps[:, seqs + i : seqs + i + 1], (8, STATE))
+                add = jnp.broadcast_to(adds[:, i : i + 1], (HEAD_DIM, STATE)) * keys[i : i + 1]
+                held = state[layer, i, h].reshape(HEAD_DIM // 8, 8, STATE)
+                new = held * keep[None] + add.reshape(HEAD_DIM // 8, 8, STATE)
+                state[layer, i, h] = new.reshape(HEAD_DIM, STATE)
+            return carry
+
+        lax.fori_loop(0, lheads // 2, update, 0)
         weight(layer, 5).wait()
+        mark("wait_m")
         for copy in copies_m:
             copy.wait_recv()
 
-        tile = min(dloc, 256)
+        mark("outproj")
+        tile = min(dloc, 1024)
 
         def project_out(j, carry, layer=layer):
             cols = pl.ds(pl.multiple_of(j * tile, tile), tile)
@@ -267,6 +329,7 @@
             return carry
 
         lax.fori_loop(0, dloc // tile, project_out, 0)
+        mark("send_o_wait")
         copies_o = []
         for k in range(1, nt):
             peer = lax.rem(tp + k, nt)
@@ -280,10 +343,12 @@
             )
             copy.start()
             copies_o.append(copy)
+        lax.fori_loop(lheads // 2, lheads * 3 // 4, update, 0)
         total = source[tp].astype(F32) + snd_o[layer, tp].astype(F32)
         for k in range(nt - 1):
             copies_o[k].wait_recv()
             total = total + rcv_o[layer, k].astype(F32)
+        mark("send_s_wait")
         stream[layer, tp] = total.astype(BF16)
         copies_s = []
         for k in range(1, nt):
@@ -297,52 +362,39 @@
             )
             copy.start()
             copies_s.append(copy)
+        lax.fori_loop(lheads * 3 // 4, lheads, update, 0)
         for copy in copies_s:
             copy.wait_recv()
+        mark("end")
         for group in (copies_e, copies_x, copies_b, copies_c, copies_z, copies_m, copies_o, copies_s):
             pending.extend(group)
 
+    mark("final")
     out_ref[...] = stream[layers - 1]
     for copy in pending:
         copy.wait_send()
-
-
-def state_kernel(
-    stream_ref, cur_ref, kept_ref, dec_ref, sx_ref, wk_ref, state_ref, out_ref, conv_ref, new_ref
-):
-    @pl.when(jnp.logical_and(pl.program_id(0) == 0, pl.program_id(1) == 0))
-    def small():
-        out_ref[...] = stream_ref[...]
-        conv_ref[:, 0 : CONV_W - 2] = kept_ref[...]
-        conv_ref[:, CONV_W - 2] = cur_ref[...]
-
-    count = state_ref.shape[1]
-    first = pl.program_id(1) * count
-    width = dec_ref.shape[2]
-    at = pl.ds(pl.multiple_of(first // 8 * 8, 8), 8)
-    layer = pl.program_id(0)
-    place = lax.rem(first, 8)
-
-    def rows_of(ref):
-        block = ref[layer, at, :]
-        rows = block[0:count]
-        for j in range(count, 8, count):
-            rows = jnp.where(place == j, block[j : j + count], rows)
-        return rows
-
-    decs, sxs, wks = rows_of(dec_ref), rows_of(sx_ref), rows_of(wk_ref)
-    for i in range(count):
-        dec = jnp.broadcast_to(decs[i : i + 1], (64, width))
-        sx = jnp.broadcast_to(sxs[i : i + 1], (64, width))
-        cols = jnp.concatenate([dec, sx], axis=0).T
-        for g in range(width // WIDTH_X):
-            part = cols[g * WIDTH_X : (g + 1) * WIDTH_X]
-            held = state_ref[0, i, g * PER_GROUP : (g + 1) * PER_GROUP].reshape(WIDTH_X, STATE)
-            write = wks[i : i + 1, g * STATE : (g + 1) * STATE]
-            new = part[:, 0:1] * held + part[:, 64:65] * write
-            new_ref[0, i, g * PER_GROUP : (g + 1) * PER_GROUP] = new.reshape(
-                PER_GROUP, HEAD_DIM, STATE
+    mark(None)
+
+
+def store_kernel(stream_ref, kept_ref, state_ref, out_ref, conv_ref, new_ref, sem):
+    layers, seqs = state_ref.shape[0:2]
+    count = 2
+    copies = [
+        pltpu.make_async_copy(stream_ref, out_ref, sem.at[0]),
+        pltpu.make_async_copy(kept_ref, conv_ref, sem.at[1]),
+    ]
+    for layer in range(layers):
+        for first in range(0, seqs, count):
+            rows = pl.ds(first, count)
+            copies.append(
+                pltpu.make_async_copy(
+                    state_ref.at[layer, rows], new_ref.at[layer, rows], sem.at[len(copies)]
+                )
             )
+    for copy in copies:
+        copy.start()
+    for copy in copies:
+        copy.wait()
 
 
 def body(
@@ -358,33 +410,40 @@
     keys = w_b.shape[2]
     turned = jnp.swapaxes(w_dt, 1, 2)
     conv_w = conv_weight.shape[2]
+    heads_all = turned.shape[1]
     vmem = pl.BlockSpec(memory_space=pltpu.VMEM)
-    anywhere = pl.BlockSpec(memory_space=pl.ANY)
+    hbm = pl.BlockSpec(memory_space=pltpu.HBM)
     dma = pltpu.SemaphoreType.DMA
     sizes = (width, keys, keys, width)
-    stream, current, kept, dec, sx, wk = pl.pallas_call(
+    past = jnp.transpose(conv_state, (0, 2, 1, 3))
+    stream, kept, new = pl.pallas_call(
         functools.partial(block_kernel, nd, nt),
         out_shape=(
-            jax.ShapeDtypeStruct((nt, rows, dloc), BF16),
-            jax.ShapeDtypeStruct((layers, seqs, conv_w), BF16),
-            jax.ShapeDtypeStruct((layers, CONV_W - 2, seqs, conv_w), BF16),
-            jax.ShapeDtypeStruct((layers, seqs, width), F32),
-            jax.ShapeDtypeStruct((layers, seqs, width), F32),
-            jax.ShapeDtypeStruct((layers, seqs, keys), F32),
+            pltpu.VMEM((nt, rows, dloc), BF16),
+            pltpu.VMEM((layers, CONV_W - 1, seqs, conv_w), BF16),
+            pltpu.VMEM(ssm_state.shape, F32),
         ),
-        in_specs=[vmem] * 9 + [anywhere] * 7,
-        out_specs=[vmem] * 6,
+        in_specs=[hbm] * 16,
+        out_specs=[vmem] * 3,
         scratch_shapes=[
+            pltpu.VMEM((nt, rows, dloc), BF16),
+            pltpu.VMEM((1, seqs), jnp.int32),
+            pltpu.VMEM(norm_gain.shape, F32),
+            pltpu.VMEM(dt_bias.shape, F32),
+            pltpu.VMEM(a_log.shape, F32),
+            pltpu.VMEM(d_skip.shape, F32),
+            pltpu.VMEM(out_gain.shape, F32),
+            pltpu.VMEM(conv_weight.shape, BF16),
+            pltpu.VMEM(past.shape, BF16),
             pltpu.VMEM(w_z.shape, BF16),
             pltpu.VMEM(w_x.shape, BF16),
             pltpu.VMEM(w_b.shape, BF16),
             pltpu.VMEM(w_c.shape, BF16),
             pltpu.VMEM(turned.shape, BF16),
             pltpu.VMEM(w_out.shape, BF16),
-            pltpu.VMEM(ssm_state.shape, F32),
-            pltpu.VMEM((layers, nd, seqs, 256), F32),
+            pltpu.VMEM((layers, nd, seqs, 2 * heads_all), F32),
             *[pltpu.VMEM((layers, nd, seqs, n), BF16) for n in sizes],
-            pltpu.VMEM((layers, nd - 1, seqs, 256), F32),
+            pltpu.VMEM((layers, nd - 1, seqs, 2 * heads_all), F32),
             *[pltpu.VMEM((layers, nd - 1, seqs, n), BF16) for n in sizes],
             pltpu.VMEM((layers, nd, seqs, width), BF16),
             pltpu.VMEM((layers, nt, rows, dloc), BF16),
@@ -393,8 +452,11 @@
             pltpu.VMEM((batch, dloc), BF16),
             pltpu.VMEM((seqs, keys), F32),
             pltpu.VMEM((seqs, width), F32),
+            pltpu.VMEM((width // WIDTH_X, seqs, STATE), F32),
+            pltpu.VMEM((width, 128), F32),
             dma((layers, 6)),
             dma((layers,)),
+            dma((9,)),
             dma((layers, 5, nd - 1)),
             dma((layers, 5, nd - 1)),
             dma((layers, nd - 1)),
@@ -405,26 +467,24 @@
             dma((layers, nt - 1)),
         ],
         compiler_params=pltpu.CompilerParams(
-            collective_id=0, has_side_effects=True, vmem_limit_bytes=56 * 1024 * 1024
+            collective_id=0, has_side_effects=True, vmem_limit_bytes=40 * 1024 * 1024
         ),
     )(
         tokens.reshape(nt, rows, dloc), lengths[None, :], norm_gain, dt_bias, a_log, d_skip,
-        out_gain, conv_weight, jnp.transpose(conv_state, (0, 2, 1, 3)),
-        w_z, w_x, w_b, w_c, turned, w_out, ssm_state,
+        out_gain, conv_weight, past, w_z, w_x, w_b, w_c, turned, w_out, ssm_state,
     )
-    step = 2
-    block = (1, step) + ssm_state.shape[2:]
     mixed_out, conv_new, ssm_new = pl.pallas_call(
-        state_kernel,
-        grid=(layers, seqs // step),
+        store_kernel,
         out_shape=(
             jax.ShapeDtypeStruct(stream.shape, BF16),
-            jax.ShapeDtypeStruct((layers, CONV_W - 1, seqs, conv_w), BF16),
+            jax.ShapeDtypeStruct(kept.shape, BF16),
             jax.ShapeDtypeStruct(ssm_state.shape, F32),
         ),
-        in_specs=[vmem] * 6 + [pl.BlockSpec(block, lambda l, s: (l, s, 0, 0, 0))],
-        out_specs=(vmem, vmem, pl.BlockSpec(block, lambda l, s: (l, s, 0, 0, 0))),
-    )(stream, current, kept, dec, sx, wk, ssm_state)
+        in_specs=[vmem] * 3,
+        out_specs=[hbm] * 3,
+        scratch_shapes=[dma((2 + layers * seqs // 2,))],
+        compiler_params=pltpu.CompilerParams(vmem_limit_bytes=1024 * 1024),
+    )(stream, kept, new)
     return mixed_out.reshape(batch, dloc), jnp.transpose(conv_new, (0, 2, 1, 3)), ssm_new
 
 

time: 73.7 us -> 52.5 us (0.71)
  Pallas kernels: 72.4 us -> 51.7 us
    pallas_call x2, Pallas kernels: 72.4 us -> 51.7 us  [the longest x1 45.6 us: body(): pl.pallas_call(functools.partial(block_kernel, nd, nt), out_shape=(pltpu....]
where the time goes in v1:
time: 52.5 us; the launch traced here: 52.4 us
  Pallas kernels  51.7 us (98%)
  between operations  0.65 us (1%)
    pallas_call x1, Pallas kernels, body(): pl.pallas_call(functools.partial(block_kernel, nd, nt), out_shape=(pltpu....  45.6 us
    pallas_call x1, Pallas kernels, body(): pl.pallas_call(store_kernel, out_shape=(jax.ShapeDtypeStruct(stream.shape...  6.15 us

profile of v1, /device:TPU:0, one launch (start us, length us, event | category | flops | bytes accessed | tf_op | source)
XLA Modules:
  0.0 52.4 jit_solution(3775443401764323008)
XLA Ops:
  0.6 45.6 %shard_map.175 = (bf16[4,16,1024]{2,1,0:T(8,128)(2,1)S(1)}, bf16[2,3,16,2048]{3,2,1,0:T(8,128)(2,1)S(1)}, f32[2,16,16,64,128]{4,3,2,1,0:T(8,128)S(1)}) custom-call(bf16[4,16,1024]{2,1,0:T(8,128)(2,1)} %bitcast.8, s32[1,16]{1,0:T(1,128)} %bitcast.9, f32[2,1024]{1,0:T(2,128)} %gain_hbm.1, f32[2,16]{1,0:T(2,128)} %bias_hbm.1, f32[2,16]{1,0:T(2,128)} %alog_hbm.1, ...), custom_call_target="tpu_custom_call" | custom-call | tf_op jit(solution)/shard_map/pallas_call | solution.py:419
  46.2 6.2 %shard_map.176 = (bf16[4,16,1024]{2,1,0:T(8,128)(2,1)}, bf16[2,3,16,2048]{3,2,1,0:T(8,128)(2,1)}, f32[2,16,16,64,128]{4,3,2,1,0:T(8,128)}) custom-call(bf16[4,16,1024]{2,1,0:T(8,128)(2,1)S(1)} %get-tuple-element.9.stream_ref, bf16[2,3,16,2048]{3,2,1,0:T(8,128)(2,1)S(1)} %get-tuple-element.10.kept_ref, f32[2,16,16,64,128]{4,3,2,1,0:T(8,128)S(1)} %get-tuple-element.11.state_ref), custom_call_target="tpu_custom_call" | custom-call | tf_op jit(solution)/shard_map/pallas_call | solution.py:476

commit v2 on v1

v2 whole, which is shorter than its diff:
```python
import functools

import jax
import jax.numpy as jnp
from jax import lax
from jax.experimental import pallas as pl
from jax.experimental.pallas import tpu as pltpu
from jax.sharding import PartitionSpec as P

D = 4096
HEADS = 64
GROUPS = 16
HEAD_DIM = 64
STATE = 128
CONV_W = 4
PER_GROUP = HEADS // GROUPS
WIDTH_X = PER_GROUP * HEAD_DIM
GROUP_W = WIDTH_X + 2 * STATE
EPSILON = 1e-06
MESH = pl.DeviceIdType.MESH
BF16 = jnp.bfloat16
F32 = jnp.float32


SCOPE = []


def mark(name):
    if SCOPE:
        SCOPE.pop().__exit__(None, None, None)
    if name:
        scope = jax.named_scope("m:" + name)
        scope.__enter__()
        SCOPE.append(scope)


def silu(t):
    return t / (1.0 + jnp.exp(-t))


def block_kernel(
    nd, nt,
    tokens_hbm, lens_hbm, gain_hbm, bias_hbm, alog_hbm, skip_hbm, ogain_hbm, taps_hbm, conv_hbm,
    wz_hbm, wx_hbm, wb_hbm, wc_hbm, wdt_hbm, wo_hbm, state_hbm,
    out_ref, kept_ref, state,
    tokens_ref, lens_ref, gain_ref, bias_ref, alog_ref, skip_ref, ogain_ref, taps_ref, conv_ref,
    wz, wx, wb, wc, wdt, wo,
    snd_e, snd_c, snd_x, snd_b, snd_z,
    rcv_e, rcv_c,
    one_x, one_b, one_z,
    two_x, two_b, two_z,
    rcv_x, rcv_b, rcv_z,
    mixes, snd_o, rcv_o, stream, acc_e, acc_c, acc_x, acc_b, acc_z, past_s, rk_s, y_s, wk_s, cols_s,
    w_sem, st_sem, in_sem, ones, oner, twos, twor, fans, fanr, rss, rsr, tgs, tgr,
):
    dp = lax.axis_index("dp")
    tp = lax.axis_index("tp")
    nx = nd // 2
    core = lax.rem(dp, 2)
    chip = dp // 2
    partner = chip * 2 + 1 - core
    layers = gain_ref.shape[0]
    seqs = lens_ref.shape[1]
    batch = nd * seqs
    rows = batch // nt
    dloc = gain_ref.shape[1]
    width = wx.shape[2]
    lgroups = width // WIDTH_X
    tile = min(dloc, 256)
    tiles = dloc // tile

    pairs = ((wdt_hbm, wdt), (wc_hbm, wc), (wx_hbm, wx), (wb_hbm, wb), (wz_hbm, wz), (wo_hbm, wo))

    def weight(layer, at):
        src, dst = pairs[at]
        return pltpu.make_async_copy(src.at[layer], dst.at[layer], w_sem.at[layer, at])

    def states(layer):
        return pltpu.make_async_copy(state_hbm.at[layer], state.at[layer], st_sem.at[layer])

    mark("start")
    arrivals = [
        pltpu.make_async_copy(src, dst, in_sem.at[i])
        for i, (src, dst) in enumerate((
            (tokens_hbm, tokens_ref), (gain_hbm, gain_ref), (lens_hbm, lens_ref),
            (bias_hbm, bias_ref), (alog_hbm, alog_ref), (skip_hbm, skip_ref),
            (ogain_hbm, ogain_ref), (taps_hbm, taps_ref), (conv_hbm, conv_ref),
        ))
    ]
    for copy in arrivals[:2]:
        copy.start()
    for at in range(5):
        weight(0, at).start()
    for copy in arrivals[2:]:
        copy.start()

    mark("barrier")
    barrier = pltpu.get_barrier_semaphore()
    for k in range(1, nd):
        pl.semaphore_signal(
            barrier, inc=1, device_id={"dp": lax.rem(dp + k, nd)}, device_id_type=MESH
        )
    for k in range(1, nt):
        pl.semaphore_signal(
            barrier, inc=1, device_id={"tp": lax.rem(tp + k, nt)}, device_id_type=MESH
        )

    streams = (
        (snd_e, None, None, rcv_e), (snd_c, None, None, rcv_c), (snd_x, one_x, two_x, rcv_x),
        (snd_b, one_b, two_b, rcv_b), (snd_z, one_z, two_z, rcv_z),
    )
    pending = []
    peers = [(k, j) for k in [*range(1, nx), 0] for j in range(2) if k or j]

    def swap(layer, at):
        snd, one = streams[at][0:2]
        copy = pltpu.make_async_remote_copy(
            src_ref=snd.at[layer, 1 - core],
            dst_ref=one.at[layer],
            send_sem=ones.at[layer, at - 2],
            recv_sem=oner.at[layer, at - 2],
            device_id={"dp": partner},
            device_id_type=MESH,
        )
        copy.start()
        pending.append(copy)
        return copy

    def relay(layer, at, swapped):
        snd, one, two, rcv = streams[at]
        swapped.wait_recv()
        copies = []
        for k in range(1, nx):
            other = lax.rem(chip + k, nx)
            summed = snd[layer, core, other].astype(F32) + one[layer, other].astype(F32)
            two[layer, k - 1] = summed.astype(two.dtype)
            copy = pltpu.make_async_remote_copy(
                src_ref=two.at[layer, k - 1],
                dst_ref=rcv.at[layer, k - 1],
                send_sem=twos.at[layer, at - 2, k - 1],
                recv_sem=twor.at[layer, at - 2, k - 1],
                device_id={"dp": other * 2 + core},
                device_id_type=MESH,
            )
            copy.start()
            copies.append(copy)
        pending.extend(copies)
        return copies

    def fan_out(layer, at, source, target):
        for i, (k, j) in enumerate(peers):
            peer_chip, peer_core = lax.rem(chip + k, nx), lax.rem(core + j, 2)
            pltpu.make_async_remote_copy(
                src_ref=source(peer_core, peer_chip),
                dst_ref=target(i),
                send_sem=fans.at[layer, at],
                recv_sem=fanr.at[layer, at],
                device_id={"dp": peer_chip * 2 + peer_core},
                device_id_type=MESH,
            ).start()

    def fanned(layer, at, ref):
        return pltpu.make_async_remote_copy(
            src_ref=ref,
            dst_ref=ref,
            send_sem=fans.at[layer, at],
            recv_sem=fanr.at[layer, at],
            device_id={"dp": partner},
            device_id_type=MESH,
        )

    def spread_out(layer, at):
        snd, rcv = streams[at][0], streams[at][3]
        fan_out(layer, at, lambda c, x: snd.at[layer, c, x], lambda i: rcv.at[layer, i])
        pending.append(fanned(layer, at, rcv.at[layer]))
        return pending[-1]

    def collected(layer, at, copy):
        snd, rcv = streams[at][0], streams[at][3]
        copy.wait_recv()
        total = snd[layer, core, chip].astype(F32)
        for i in range(nd - 1):
            total = total + rcv[layer, i].astype(F32)
        return total

    def gathered(layer, at, copies):
        snd, one, two, rcv = streams[at]
        total = snd[layer, core, chip].astype(F32) + one[layer, chip].astype(F32)
        for k in range(nx - 1):
            copies[k].wait_recv()
            total = total + rcv[layer, k].astype(F32)
        return total

    def far_first(k):
        down = nt - 1 - k
        down = jnp.where(down > tp, down, down - 1)
        up = jnp.where(k < tp, k, k + 1)
        return jnp.where(2 * tp < nt, down, up)

    def tp_copy(src, dst, sems, layer, q, peer):
        return pltpu.make_async_remote_copy(
            src_ref=src,
            dst_ref=dst,
            send_sem=sems[0].at[layer],
            recv_sem=sems[1].at[layer, q],
            device_id={"tp": peer},
            device_id_type=MESH,
        )

    def send_sums(layer, q):
        for k in range(nt - 1):
            peer = far_first(k)
            slot = lax.rem(tp + nt - peer, nt) - 1
            tp_copy(
                snd_o.at[layer, q, peer], rcv_o.at[layer, q, slot], (rss, rsr), layer, q, peer
            ).start()

    def wait_sums(layer, q):
        held = rcv_o.at[layer, q]
        tp_copy(held, held, (rss, rsr), layer, q, 0).wait_recv()

    def send_rows(layer, q):
        mine = stream.at[layer, q, tp]
        for k in range(nt - 1):
            tp_copy(mine, mine, (tgs, tgr), layer, q, far_first(k)).start()

    def wait_rows(layer, q):
        held = stream.at[layer, q, 0 : nt - 1]
        tp_copy(held, held, (tgs, tgr), layer, q, 0).wait_recv()

    mark("prep")
    for copy in arrivals[:2]:
        copy.wait()
    states(0).start()
    weight(0, 5).start()
    heads_all = wdt.shape[1]
    lheads = bias_ref.shape[1]

    def expand(values, offset):
        count = values.shape[1]
        head = lax.broadcasted_iota(jnp.int32, (count, width), 0)
        lane = lax.broadcasted_iota(jnp.int32, (count, width), 1)
        pick = jnp.where(head == lane // HEAD_DIM + offset, 1.0, 0.0).astype(F32)
        return jnp.dot(
            values, pick, preferred_element_type=F32, precision=lax.Precision.HIGHEST
        )

    for layer in range(layers):
        mark("project")
        squares = None
        last = tiles - 1 if layer else 0
        for q in range(last + 1):
            if layer:
                wait_rows(layer - 1, q)
                size = tile
                wide = stream[layer - 1, q].astype(F32).reshape(batch, size)
            else:
                size = dloc
                wide = tokens_ref[...].astype(F32).reshape(batch, size)
            feats = slice(q * size, (q + 1) * size)
            square = jnp.sum(wide * wide, axis=-1, keepdims=True)
            squares = square if q == 0 else squares + square
            lhs = (wide * gain_ref[layer : layer + 1, feats]).astype(BF16)

            def store(part, snd):
                for d in range(nd):
                    snd[layer, d % 2, d // 2] = part[d * seqs : (d + 1) * seqs].astype(snd.dtype)

            def project(at, w_ref, acc, snd):
                if q == 0:
                    weight(layer, at).wait()
                part = jnp.dot(lhs, w_ref[layer, feats, :], preferred_element_type=F32)
                if q:
                    part = part + acc[...]
                if q < last:
                    acc[...] = part
                else:
                    store(part, snd)

            project(1, wc, acc_c, snd_c)
            if q == last and layer:
                copies_c = spread_out(layer, 1)
            if q == 0:
                weight(layer, 0).wait()
            part = lax.dot_general(
                lhs, wdt[layer, :, feats], (((1,), (1,)), ((), ())), preferred_element_type=F32
            )
            if q:
                part = part + acc_e[...]
            if q < last:
                acc_e[...] = part
            else:
                total = jnp.broadcast_to(squares, (batch, heads_all))
                store(jnp.concatenate([part, total], axis=1), snd_e)
                if layer:
                    copies_e = spread_out(layer, 0)
            project(2, wx, acc_x, snd_x)
            if q == last and layer:
                swap_x = swap(layer, 2)
            project(3, wb, acc_b, snd_b)
            if q == last:
                if layer == 0:
                    pl.semaphore_wait(barrier, nd - 1 + nt - 1)
                    copies_c = spread_out(layer, 1)
                    copies_e = spread_out(layer, 0)
                    swap_x = swap(layer, 2)
                swap_b = swap(layer, 3)
            project(4, wz, acc_z, snd_z)
            if q == last:
                swap_z = swap(layer, 4)
        mark("relay_xbz")
        copies_x = relay(layer, 2, swap_x)
        copies_b = relay(layer, 3, swap_b)
        copies_z = relay(layer, 4, swap_z)
        mark("history")
        if layer + 1 < layers:
            for at in range(6):
                weight(layer + 1, at).start()
            states(layer + 1).start()
        if layer == 0:
            for copy in arrivals[2:]:
                copy.wait()
            bias = expand(bias_ref[...], 0)
            rate = jnp.exp(expand(alog_ref[...], 0))
            skip = expand(skip_ref[...], 0)
            spread = jnp.broadcast_to(lens_ref[...].astype(F32), (seqs, seqs))
            diagonal = lax.broadcasted_iota(jnp.int32, (seqs, seqs), 0) == lax.broadcasted_iota(
                jnp.int32, (seqs, seqs), 1
            )
            lens = jnp.sum(jnp.where(diagonal, spread, 0.0), axis=1, keepdims=True)
        summed = None
        for tap in range(CONV_W - 1):
            past = conv_ref[layer, tap].astype(F32)
            past = jnp.where(lens >= CONV_W - tap, past, 0.0)
            if tap >= 1:
                kept_ref[layer, tap - 1] = past.astype(BF16)
            past = past * taps_ref[layer, tap : tap + 1, :].astype(F32)
            summed = past if tap == 0 else summed + past
        past_s[...] = summed

        def convolve(current, first, size, layer=layer):
            found = []
            for g in range(lgroups):
                cols = slice(g * GROUP_W + first, g * GROUP_W + first + size)
                part = current[:, g * size : (g + 1) * size]
                kept_ref[layer, CONV_W - 2, :, cols] = part
                tap = taps_ref[layer, CONV_W - 1 : CONV_W, cols].astype(F32)
                found.append(silu(part.astype(F32) * tap + past_s[:, cols]))
            return found

        if layer:
            mark("update3")
            lax.fori_loop(lheads * 3 // 4, lheads, functools.partial(update, layer=layer - 1), 0)
        mark("wait_e")
        extra = collected(layer, 0, copies_e)
        inverse = lax.rsqrt(extra[:, heads_all : heads_all + 1] / D + EPSILON)
        raw = expand(extra[:, 0:heads_all] * inverse, tp * lheads)
        softin = raw + bias[layer : layer + 1, :]
        step = jnp.maximum(softin, 0.0) + jnp.log1p(jnp.exp(-jnp.abs(softin)))
        decay = jnp.exp(-rate[layer : layer + 1, :] * step)
        decay = jnp.where(lens >= 2, decay, 0.0)

        mark("wait_c")
        reads = (collected(layer, 1, copies_c) * inverse).astype(BF16)
        rk = convolve(reads, WIDTH_X + STATE, STATE)
        rk_s[...] = jnp.concatenate(rk, axis=1)
        mark("wait_state")
        states(layer).wait()

        mark("readout")
        def read_eight(b, carry, layer=layer):
            at = pl.ds(pl.multiple_of(b * 8, 8), 8)
            keys = rk_s[at, :]
            lines = []
            for i in range(8):
                outs = []
                for g in range(lgroups):
                    row = keys[i : i + 1, g * STATE : (g + 1) * STATE]
                    lhs = jnp.broadcast_to(row, (16, STATE)).astype(BF16)
                    held = state[layer, b * 8 + i, g * PER_GROUP : (g + 1) * PER_GROUP]
                    held = held.reshape(WIDTH_X, STATE).astype(BF16)
                    res = lax.dot_general(
                        lhs, held, (((1,), (1,)), ((), ())), preferred_element_type=F32
                    )
                    outs.append(res[0:1])
                lines.append(jnp.concatenate(outs, axis=1))
            y_s[at, :] = jnp.concatenate(lines, axis=0)
            return carry

        lax.fori_loop(0, seqs // 8, read_eight, 0)
        mark("wait_xb")
        values = (gathered(layer, 2, copies_x) * inverse).astype(BF16)
        head_in = jnp.concatenate(convolve(values, 0, WIDTH_X), axis=1)
        stepx = step * head_in
        writes = (gathered(layer, 3, copies_b) * inverse).astype(BF16)
        wk = convolve(writes, WIDTH_X, STATE)
        for g in range(lgroups):
            wk_s[g] = wk[g]
        mark("wait_z_gate")
        readout = decay * y_s[...] + skip[layer : layer + 1, :] * head_in
        gate = (gathered(layer, 4, copies_z) * inverse).astype(BF16).astype(F32)
        gate = silu(gate)
        mixed = []
        for g in range(lgroups):
            cols = slice(g * WIDTH_X, (g + 1) * WIDTH_X)
            cross = jnp.sum(wk[g] * rk[g], axis=-1, keepdims=True)
            gated = (readout[:, cols] + stepx[:, cols] * cross) * gate[:, cols]
            norm = lax.rsqrt(jnp.mean(gated * gated, axis=-1, keepdims=True) + EPSILON)
            mixed.append(gated * norm * ogain_ref[layer : layer + 1, cols])
        mixes[layer, dp] = jnp.concatenate(mixed, axis=1).astype(BF16)
        mark("send_m")
        mine = mixes.at[layer, dp]
        fan_out(layer, 2, lambda c, x: mine, lambda i: mine)
        copy_m = fanned(layer, 2, mixes.at[layer, 0 : nd - 1])
        pending.append(copy_m)
        mark("update")
        cols_s[...] = jnp.concatenate(
            [stepx, decay, jnp.zeros((128 - 2 * seqs, width), F32)], axis=0
        ).T

        def update(h, carry, layer=layer):
            first = pl.multiple_of(h * HEAD_DIM, HEAD_DIM)
            adds = cols_s[pl.ds(first, HEAD_DIM), :]
            keeps = cols_s[pl.ds(first, 8), :]
            keys = wk_s[h // PER_GROUP]
            for i in range(seqs):
                keep = jnp.broadcast_to(keeps[:, seqs + i : seqs + i + 1], (8, STATE))
                add = jnp.broadcast_to(adds[:, i : i + 1], (HEAD_DIM, STATE)) * keys[i : i + 1]
                held = state[layer, i, h].reshape(HEAD_DIM // 8, 8, STATE)
                new = held * keep[None] + add.reshape(HEAD_DIM // 8, 8, STATE)
                state[layer, i, h] = new.reshape(HEAD_DIM, STATE)
            return carry

        lax.fori_loop(0, lheads // 2, update, 0)
        weight(layer, 5).wait()
        mark("wait_m")
        copy_m.wait_recv()

        mark("outproj")
        lhs = mixes[layer].reshape(batch, width)
        for q in range(tiles):
            feats = slice(q * tile, (q + 1) * tile)
            part = jnp.dot(lhs, wo[layer, :, feats], preferred_element_type=F32)
            snd_o[layer, q] = part.reshape(nt, rows, tile).astype(BF16)
            send_sums(layer, q)
        mark("update2")
        lax.fori_loop(lheads // 2, lheads * 3 // 4, update, 0)
        mark("wait_o")
        for q in range(tiles):
            if layer:
                total = stream[layer - 1, q, tp].astype(F32)
            else:
                total = tokens_ref[tp, :, q * tile : (q + 1) * tile].astype(F32)
            total = total + snd_o[layer, q, tp].astype(F32)
            wait_sums(layer, q)
            for k in range(nt - 1):
                total = total + rcv_o[layer, q, k].astype(F32)
            stream[layer, q, tp] = total.astype(BF16)
            send_rows(layer, q)
        if layer + 1 == layers:
            mark("update3")
            lax.fori_loop(lheads * 3 // 4, lheads, update, 0)

    mark("wait_s")
    for q in range(tiles):
        wait_rows(layers - 1, q)
        out_ref[:, :, q * tile : (q + 1) * tile] = stream[layers - 1, q]
    mark("final")
    for copy in pending:
        copy.wait_send()
    for layer in range(layers):
        for ref, sems in ((snd_o, (rss, rsr)), (stream, (tgs, tgr))):
            held = ref.at[layer, :, 0 : nt - 1]
            tp_copy(held, held, sems, layer, 0, 0).wait_send()
    mark(None)


def store_kernel(stream_ref, kept_ref, state_ref, out_ref, conv_ref, new_ref, sem):
    layers, seqs = state_ref.shape[0:2]
    count = 4
    for layer in range(layers):
        for first in range(0, seqs, count):
            rows = pl.ds(first, count)
            pltpu.make_async_copy(
                state_ref.at[layer, rows], new_ref.at[layer, rows], sem.at[0]
            ).start()
    copies = [
        pltpu.make_async_copy(stream_ref, out_ref, sem.at[1]),
        pltpu.make_async_copy(kept_ref, conv_ref, sem.at[2]),
    ]
    for copy in copies:
        copy.start()
    for copy in copies:
        copy.wait()
    pltpu.make_async_copy(state_ref, new_ref, sem.at[0]).wait()


def body(
    nd, nt,
    tokens, lengths, norm_gain, w_z, w_x, w_b, w_c, w_dt, conv_weight,
    dt_bias, a_log, d_skip, out_gain, w_out, conv_state, ssm_state,
):
    layers = w_z.shape[0]
    batch, dloc = tokens.shape
    seqs = lengths.shape[0]
    rows = batch // nt
    width = w_x.shape[2]
    keys = w_b.shape[2]
    turned = jnp.swapaxes(w_dt, 1, 2)
    conv_w = conv_weight.shape[2]
    heads_all = turned.shape[1]
    vmem = pl.BlockSpec(memory_space=pltpu.VMEM)
    hbm = pl.BlockSpec(memory_space=pltpu.HBM)
    dma = pltpu.SemaphoreType.DMA
    nx = nd // 2
    tile = min(dloc, 256)
    tiles = dloc // tile

    def parts(*lead):
        shapes = [(layers, *lead, seqs, n) for n in (2 * heads_all, keys, width, keys, width)]
        return [pltpu.VMEM(shape, BF16 if i else F32) for i, shape in enumerate(shapes)]

    past = jnp.transpose(conv_state, (0, 2, 1, 3))
    stream, kept, new = pl.pallas_call(
        functools.partial(block_kernel, nd, nt),
        out_shape=(
            pltpu.VMEM((nt, rows, dloc), BF16),
            pltpu.VMEM((layers, CONV_W - 1, seqs, conv_w), BF16),
            pltpu.VMEM(ssm_state.shape, F32),
        ),
        in_specs=[hbm] * 16,
        out_specs=[vmem] * 3,
        scratch_shapes=[
            pltpu.VMEM((nt, rows, dloc), BF16),
            pltpu.VMEM((1, seqs), jnp.int32),
            pltpu.VMEM(norm_gain.shape, F32),
            pltpu.VMEM(dt_bias.shape, F32),
            pltpu.VMEM(a_log.shape, F32),
            pltpu.VMEM(d_skip.shape, F32),
            pltpu.VMEM(out_gain.shape, F32),
            pltpu.VMEM(conv_weight.shape, BF16),
            pltpu.VMEM(past.shape, BF16),
            pltpu.VMEM(w_z.shape, BF16),
            pltpu.VMEM(w_x.shape, BF16),
            pltpu.VMEM(w_b.shape, BF16),
            pltpu.VMEM(w_c.shape, BF16),
            pltpu.VMEM(turned.shape, BF16),
            pltpu.VMEM(w_out.shape, BF16),
            *parts(2, nx),
            *parts(nd - 1)[:2],
            *parts(nx)[2:],
            *parts(max(nx - 1, 1))[2:],
            *parts(max(nx - 1, 1))[2:],
            pltpu.VMEM((layers, nd, seqs, width), BF16),
            *[pltpu.VMEM((layers, tiles, n, rows, tile), BF16) for n in (nt, nt - 1, nt)],
            *[pltpu.VMEM((batch, n), F32) for n in (heads_all, keys, width, keys, width)],
            pltpu.VMEM((seqs, conv_w), F32),
            pltpu.VMEM((seqs, keys), F32),
            pltpu.VMEM((seqs, width), F32),
            pltpu.VMEM((width // WIDTH_X, seqs, STATE), F32),
            pltpu.VMEM((width, 128), F32),
            dma((layers, 6)),
            dma((layers,)),
            dma((9,)),
            dma((layers, 3)),
            dma((layers, 3)),
            dma((layers, 3, max(nx - 1, 1))),
            dma((layers, 3, max(nx - 1, 1))),
            dma((layers, 3)),
            dma((layers, 3)),
            dma((layers,)),
            dma((layers, tiles)),
            dma((layers,)),
            dma((layers, tiles)),
        ],
        compiler_params=pltpu.CompilerParams(
            collective_id=0, has_side_effects=True, vmem_limit_bytes=40 * 1024 * 1024
        ),
    )(
        tokens.reshape(nt, rows, dloc), lengths[None, :], norm_gain, dt_bias, a_log, d_skip,
        out_gain, conv_weight, past, w_z, w_x, w_b, w_c, turned, w_out, ssm_state,
    )
    mixed_out, conv_new, ssm_new = pl.pallas_call(
        store_kernel,
        out_shape=(
            jax.ShapeDtypeStruct(stream.shape, BF16),
            jax.ShapeDtypeStruct(kept.shape, BF16),
            jax.ShapeDtypeStruct(ssm_state.shape, F32),
        ),
        in_specs=[vmem] * 3,
        out_specs=[hbm] * 3,
        scratch_shapes=[dma((3,))],
        compiler_params=pltpu.CompilerParams(vmem_limit_bytes=1024 * 1024),
    )(stream, kept, new)
    return mixed_out.reshape(batch, dloc), jnp.transpose(conv_new, (0, 2, 1, 3)), ssm_new


def solution(mesh):
    placed = (
        P("grp", "dp"),
        P(("grp", "dp")),
        P(None, "dp"),
        P(None, "dp", "tp"),
        P(None, "dp", "tp"),
        P(None, "dp", "tp"),
        P(None, "dp", "tp"),
        P(None, "dp", None),
        P(None, None, "tp"),
        P(None, "tp"),
        P(None, "tp"),
        P(None, "tp"),
        P(None, "tp"),
        P(None, "tp", "dp"),
        P(None, ("grp", "dp"), None, "tp"),
        P(None, ("grp", "dp"), "tp", None, None),
    )
    return jax.shard_map(
        functools.partial(body, mesh.shape["dp"], mesh.shape["tp"]),
        mesh=mesh,
        in_specs=placed,
        out_specs=(
            P("grp", "dp"),
            P(None, ("grp", "dp"), None, "tp"),
            P(None, ("grp", "dp"), "tp", None, None),
        ),
        check_vma=False,
    )
```

time: 52.5 us -> 48 us (0.914)
  Pallas kernels: 51.7 us -> 47.2 us
    pallas_call x1, Pallas kernels: 45.6 us -> 41.3 us  [body(): pl.pallas_call(functools.partial(block_kernel, nd, nt), out_shape=(pltpu....]
where the time goes in v2:
time: 48 us; the launch traced here: 47.9 us
  Pallas kernels  47.2 us (98%)
  between operations  0.65 us (1%)
    pallas_call x1, Pallas kernels, body(): pl.pallas_call(functools.partial(block_kernel, nd, nt), out_shape=(pltpu....  41.3 us
    pallas_call x1, Pallas kernels, body(): pl.pallas_call(store_kernel, out_shape=(jax.ShapeDtypeStruct(stream.shape...  5.98 us

profile of v2, /device:TPU:0, one launch (start us, length us, event | category | flops | bytes accessed | tf_op | source)
XLA Modules:
  0.0 47.9 jit_solution(12395586373816974762)
XLA Ops:
  0.6 41.3 %shard_map.175 = (bf16[4,16,1024]{2,1,0:T(8,128)(2,1)S(1)}, bf16[2,3,16,2048]{3,2,1,0:T(8,128)(2,1)S(1)}, f32[2,16,16,64,128]{4,3,2,1,0:T(8,128)S(1)}) custom-call(bf16[4,16,1024]{2,1,0:T(8,128)(2,1)} %bitcast.8, s32[1,16]{1,0:T(1,128)} %bitcast.9, f32[2,1024]{1,0:T(2,128)} %gain_hbm.1, f32[2,16]{1,0:T(2,128)} %bias_hbm.1, f32[2,16]{1,0:T(2,128)} %alog_hbm.1, ...), custom_call_target="tpu_custom_call" | custom-call | tf_op jit(solution)/shard_map/pallas_call | solution.py:524
  41.9 6.0 %shard_map.176 = (bf16[4,16,1024]{2,1,0:T(8,128)(2,1)}, bf16[2,3,16,2048]{3,2,1,0:T(8,128)(2,1)}, f32[2,16,16,64,128]{4,3,2,1,0:T(8,128)}) custom-call(bf16[4,16,1024]{2,1,0:T(8,128)(2,1)S(1)} %get-tuple-element.9.stream_ref, bf16[2,3,16,2048]{3,2,1,0:T(8,128)(2,1)S(1)} %get-tuple-element.10.kept_ref, f32[2,16,16,64,128]{4,3,2,1,0:T(8,128)S(1)} %get-tuple-element.11.state_ref), custom_call_target="tpu_custom_call" | custom-call | tf_op jit(solution)/shard_map/pallas_call | solution.py:583

commit v3 on v2

--- a/solution.py
+++ b/solution.py
@@ -50,7 +50,7 @@
     one_x, one_b, one_z,
     two_x, two_b, two_z,
     rcv_x, rcv_b, rcv_z,
-    mixes, snd_o, rcv_o, stream, acc_e, acc_c, acc_x, acc_b, acc_z, past_s, rk_s, y_s, wk_s, cols_s,
+    mixes, snd_o, rcv_o, stream, acc_e, acc_c, acc_x, acc_b, acc_z, past_s, wk_s, cols_s,
     w_sem, st_sem, in_sem, ones, oner, twos, twor, fans, fanr, rss, rsr, tgs, tgr,
 ):
     dp = lax.axis_index("dp")
@@ -62,7 +62,11 @@
     layers = gain_ref.shape[0]
     seqs = lens_ref.shape[1]
     batch = nd * seqs
-    rows = batch // nt
+    half = batch // 2
+    first_owner = nt // 2 - 1
+    own = tp - first_owner
+    owner = jnp.logical_and(own >= 0, own < 2)
+    far = jnp.where(2 * tp < nt, 1, 0)
     dloc = gain_ref.shape[1]
     width = wx.shape[2]
     lgroups = width // WIDTH_X
@@ -73,7 +77,7 @@
 
     def weight(layer, at):
         src, dst = pairs[at]
-        return pltpu.make_async_copy(src.at[layer], dst.at[layer], w_sem.at[layer, at])
+        return pltpu.make_async_copy(src.at[layer], dst.at[layer], w_sem.at[at if at < 5 else at + layer])
 
     def states(layer):
         return pltpu.make_async_copy(state_hbm.at[layer], state.at[layer], st_sem.at[layer])
@@ -100,34 +104,60 @@
         pl.semaphore_signal(
             barrier, inc=1, device_id={"dp": lax.rem(dp + k, nd)}, device_id_type=MESH
         )
-    for k in range(1, nt):
-        pl.semaphore_signal(
-            barrier, inc=1, device_id={"tp": lax.rem(tp + k, nt)}, device_id_type=MESH
-        )
+    for i in range(2):
+
+        @pl.when(own != i)
+        def greet(i=i):
+            pl.semaphore_signal(
+                barrier, inc=1, device_id={"tp": first_owner + i}, device_id_type=MESH
+            )
+
+    for peer in (*range(first_owner), *range(first_owner + 2, nt)):
+
+        @pl.when(owner)
+        def answer(peer=peer):
+            pl.semaphore_signal(barrier, inc=1, device_id={"tp": peer}, device_id_type=MESH)
+
+
+    def hear_all():
+        @pl.when(owner)
+        def heard_all():
+            pl.semaphore_wait(barrier, nd - 1 + nt - 1)
+
+        @pl.when(jnp.logical_not(owner))
+        def heard_owners():
+            pl.semaphore_wait(barrier, nd - 1 + 2)
 
     streams = (
         (snd_e, None, None, rcv_e), (snd_c, None, None, rcv_c), (snd_x, one_x, two_x, rcv_x),
         (snd_b, one_b, two_b, rcv_b), (snd_z, one_z, two_z, rcv_z),
     )
-    pending = []
+    flying = {}
     peers = [(k, j) for k in [*range(1, nx), 0] for j in range(2) if k or j]
+
+    def settle(key, copies):
+        for copy in flying.pop(key, ()):
+            copy.wait_send()
+        if copies:
+            flying[key] = copies
 
     def swap(layer, at):
         snd, one = streams[at][0:2]
         copy = pltpu.make_async_remote_copy(
             src_ref=snd.at[layer, 1 - core],
             dst_ref=one.at[layer],
-            send_sem=ones.at[layer, at - 2],
-            recv_sem=oner.at[layer, at - 2],
+            send_sem=ones.at[at - 2],
+            recv_sem=oner.at[at - 2],
             device_id={"dp": partner},
             device_id_type=MESH,
         )
+        settle(("swap", at), [copy])
         copy.start()
-        pending.append(copy)
         return copy
 
     def relay(layer, at, swapped):
         snd, one, two, rcv = streams[at]
+        settle(("relay", at), [])
         swapped.wait_recv()
         copies = []
         for k in range(1, nx):
@@ -137,43 +167,43 @@
             copy = pltpu.make_async_remote_copy(
                 src_ref=two.at[layer, k - 1],
                 dst_ref=rcv.at[layer, k - 1],
-                send_sem=twos.at[layer, at - 2, k - 1],
-                recv_sem=twor.at[layer, at - 2, k - 1],
+                send_sem=twos.at[at - 2, k - 1],
+                recv_sem=twor.at[at - 2, k - 1],
                 device_id={"dp": other * 2 + core},
                 device_id_type=MESH,
             )
             copy.start()
             copies.append(copy)
-        pending.extend(copies)
+        flying["relay", at] = copies
         return copies
 
-    def fan_out(layer, at, source, target):
+    def fan_out(at, ref, source, target):
+        settle(("fan", at), [fanned(at, ref)])
         for i, (k, j) in enumerate(peers):
             peer_chip, peer_core = lax.rem(chip + k, nx), lax.rem(core + j, 2)
             pltpu.make_async_remote_copy(
                 src_ref=source(peer_core, peer_chip),
                 dst_ref=target(i),
-                send_sem=fans.at[layer, at],
-                recv_sem=fanr.at[layer, at],
+                send_sem=fans.at[at],
+                recv_sem=fanr.at[at],
                 device_id={"dp": peer_chip * 2 + peer_core},
                 device_id_type=MESH,
             ).start()
 
-    def fanned(layer, at, ref):
+    def fanned(at, ref):
         return pltpu.make_async_remote_copy(
             src_ref=ref,
             dst_ref=ref,
-            send_sem=fans.at[layer, at],
-            recv_sem=fanr.at[layer, at],
+            send_sem=fans.at[at],
+            recv_sem=fanr.at[at],
             device_id={"dp": partner},
             device_id_type=MESH,
         )
 
     def spread_out(layer, at):
         snd, rcv = streams[at][0], streams[at][3]
-        fan_out(layer, at, lambda c, x: snd.at[layer, c, x], lambda i: rcv.at[layer, i])
-        pending.append(fanned(layer, at, rcv.at[layer]))
-        return pending[-1]
+        fan_out(at, rcv.at[layer], lambda c, x: snd.at[layer, c, x], lambda i: rcv.at[layer, i])
+        return fanned(at, rcv.at[layer])
 
     def collected(layer, at, copy):
         snd, rcv = streams[at][0], streams[at][3]
@@ -197,36 +227,58 @@
         up = jnp.where(k < tp, k, k + 1)
         return jnp.where(2 * tp < nt, down, up)
 
-    def tp_copy(src, dst, sems, layer, q, peer):
+    def tp_copy(src, dst, send, recv, peer):
         return pltpu.make_async_remote_copy(
             src_ref=src,
             dst_ref=dst,
-            send_sem=sems[0].at[layer],
-            recv_sem=sems[1].at[layer, q],
+            send_sem=send,
+            recv_sem=recv,
             device_id={"tp": peer},
             device_id_type=MESH,
         )
 
     def send_sums(layer, q):
-        for k in range(nt - 1):
-            peer = far_first(k)
-            slot = lax.rem(tp + nt - peer, nt) - 1
-            tp_copy(
-                snd_o.at[layer, q, peer], rcv_o.at[layer, q, slot], (rss, rsr), layer, q, peer
-            ).start()
+        for i in (far, 1 - far):
+
+            @pl.when(own != i)
+            def send(i=i):
+                peer = first_owner + i
+                slot = lax.rem(tp + nt - peer, nt) - 1
+                tp_copy(
+                    snd_o.at[layer, q, i], rcv_o.at[layer, q, slot],
+                    rss.at[i], rsr.at[q], peer,
+                ).start()
+
+    def sent_sums(layer):
+        for i in range(2):
+
+            @pl.when(own != i)
+            def sent(i=i):
+                held = snd_o.at[layer, :, i]
+                tp_copy(held, held, rss.at[i], rsr.at[0], 0).wait_send()
+
+    def sent_rows(layer):
+        @pl.when(owner)
+        def sent():
+            held = rcv_o.at[layer]
+            tp_copy(held, held, tgs.at[0], tgr.at[0, 0], 0).wait_send()
 
     def wait_sums(layer, q):
         held = rcv_o.at[layer, q]
-        tp_copy(held, held, (rss, rsr), layer, q, 0).wait_recv()
+        tp_copy(held, held, rss.at[0], rsr.at[q], 0).wait_recv()
 
     def send_rows(layer, q):
-        mine = stream.at[layer, q, tp]
+        mine = stream.at[layer, q, own]
         for k in range(nt - 1):
-            tp_copy(mine, mine, (tgs, tgr), layer, q, far_first(k)).start()
+            tp_copy(mine, mine, tgs.at[0], tgr.at[q, own], far_first(k)).start()
 
     def wait_rows(layer, q):
-        held = stream.at[layer, q, 0 : nt - 1]
-        tp_copy(held, held, (tgs, tgr), layer, q, 0).wait_recv()
+        for i in range(2):
+
+            @pl.when(own != i)
+            def wait(i=i):
+                held = stream.at[layer, q, i]
+                tp_copy(held, held, tgs.at[0], tgr.at[q, i], 0).wait_recv()
 
     mark("prep")
     for copy in arrivals[:2]:
@@ -292,18 +344,15 @@
             else:
                 total = jnp.broadcast_to(squares, (batch, heads_all))
                 store(jnp.concatenate([part, total], axis=1), snd_e)
-                if layer:
-                    copies_e = spread_out(layer, 0)
+                if layer == 0:
+                    hear_all()
+                    copies_c = spread_out(layer, 1)
+                copies_e = spread_out(layer, 0)
             project(2, wx, acc_x, snd_x)
-            if q == last and layer:
+            if q == last:
                 swap_x = swap(layer, 2)
             project(3, wb, acc_b, snd_b)
             if q == last:
-                if layer == 0:
-                    pl.semaphore_wait(barrier, nd - 1 + nt - 1)
-                    copies_c = spread_out(layer, 1)
-                    copies_e = spread_out(layer, 0)
-                    swap_x = swap(layer, 2)
                 swap_b = swap(layer, 3)
             project(4, wz, acc_z, snd_z)
             if q == last:
@@ -363,31 +412,27 @@
         mark("wait_c")
         reads = (collected(layer, 1, copies_c) * inverse).astype(BF16)
         rk = convolve(reads, WIDTH_X + STATE, STATE)
-        rk_s[...] = jnp.concatenate(rk, axis=1)
         mark("wait_state")
         states(layer).wait()
 
-        mark("readout")
-        def read_eight(b, carry, layer=layer):
-            at = pl.ds(pl.multiple_of(b * 8, 8), 8)
-            keys = rk_s[at, :]
+        def read_eight(first, layer=layer):
             lines = []
-            for i in range(8):
+            for i in range(first, first + 8):
                 outs = []
                 for g in range(lgroups):
-                    row = keys[i : i + 1, g * STATE : (g + 1) * STATE]
+                    row = rk[g][i : i + 1]
                     lhs = jnp.broadcast_to(row, (16, STATE)).astype(BF16)
-                    held = state[layer, b * 8 + i, g * PER_GROUP : (g + 1) * PER_GROUP]
+                    held = state[layer, i, g * PER_GROUP : (g + 1) * PER_GROUP]
                     held = held.reshape(WIDTH_X, STATE).astype(BF16)
                     res = lax.dot_general(
                         lhs, held, (((1,), (1,)), ((), ())), preferred_element_type=F32
                     )
                     outs.append(res[0:1])
                 lines.append(jnp.concatenate(outs, axis=1))
-            y_s[at, :] = jnp.concatenate(lines, axis=0)
-            return carry
-
-        lax.fori_loop(0, seqs // 8, read_eight, 0)
+            return jnp.concatenate(lines, axis=0)
+
+        mark("readout")
+        found = [read_eight(first) for first in range(0, seqs, 8)]
         mark("wait_xb")
         values = (gathered(layer, 2, copies_x) * inverse).astype(BF16)
         head_in = jnp.concatenate(convolve(values, 0, WIDTH_X), axis=1)
@@ -396,23 +441,24 @@
         wk = convolve(writes, WIDTH_X, STATE)
         for g in range(lgroups):
             wk_s[g] = wk[g]
-        mark("wait_z_gate")
-        readout = decay * y_s[...] + skip[layer : layer + 1, :] * head_in
+        mark("wait_z")
         gate = (gathered(layer, 4, copies_z) * inverse).astype(BF16).astype(F32)
         gate = silu(gate)
-        mixed = []
-        for g in range(lgroups):
-            cols = slice(g * WIDTH_X, (g + 1) * WIDTH_X)
-            cross = jnp.sum(wk[g] * rk[g], axis=-1, keepdims=True)
-            gated = (readout[:, cols] + stepx[:, cols] * cross) * gate[:, cols]
-            norm = lax.rsqrt(jnp.mean(gated * gated, axis=-1, keepdims=True) + EPSILON)
-            mixed.append(gated * norm * ogain_ref[layer : layer + 1, cols])
-        mixes[layer, dp] = jnp.concatenate(mixed, axis=1).astype(BF16)
-        mark("send_m")
-        mine = mixes.at[layer, dp]
-        fan_out(layer, 2, lambda c, x: mine, lambda i: mine)
-        copy_m = fanned(layer, 2, mixes.at[layer, 0 : nd - 1])
-        pending.append(copy_m)
+        for part_at in range(seqs // 8):
+            at = slice(part_at * 8, part_at * 8 + 8)
+            mark("gate")
+            readout = decay[at] * found[part_at] + skip[layer : layer + 1, :] * head_in[at]
+            mixed = []
+            for g in range(lgroups):
+                cols = slice(g * WIDTH_X, (g + 1) * WIDTH_X)
+                cross = jnp.sum(wk[g][at] * rk[g][at], axis=-1, keepdims=True)
+                gated = (readout[:, cols] + stepx[at, cols] * cross) * gate[at, cols]
+                norm = lax.rsqrt(jnp.mean(gated * gated, axis=-1, keepdims=True) + EPSILON)
+                mixed.append(gated * norm * ogain_ref[layer : layer + 1, cols])
+            mixes[layer, part_at, dp] = jnp.concatenate(mixed, axis=1).astype(BF16)
+            mine = mixes.at[layer, part_at, dp]
+            others = mixes.at[layer, part_at, 0 : nd - 1]
+            fan_out(2 + part_at, others, lambda c, x, mine=mine: mine, lambda i, mine=mine: mine)
         mark("update")
         cols_s[...] = jnp.concatenate(
             [stepx, decay, jnp.zeros((128 - 2 * seqs, width), F32)], axis=0
@@ -434,29 +480,45 @@
         lax.fori_loop(0, lheads // 2, update, 0)
         weight(layer, 5).wait()
         mark("wait_m")
-        copy_m.wait_recv()
+        for part_at in range(seqs // 8):
+            fanned(2 + part_at, mixes.at[layer, part_at, 0 : nd - 1]).wait_recv()
 
         mark("outproj")
+        if layer:
+            sent_sums(layer - 1)
+            sent_rows(layer - 1)
         lhs = mixes[layer].reshape(batch, width)
         for q in range(tiles):
             feats = slice(q * tile, (q + 1) * tile)
             part = jnp.dot(lhs, wo[layer, :, feats], preferred_element_type=F32)
-            snd_o[layer, q] = part.reshape(nt, rows, tile).astype(BF16)
+            part = jnp.concatenate(
+                [
+                    part[(j * nd + d) * 8 : (j * nd + d) * 8 + 8]
+                    for d in range(nd)
+                    for j in range(seqs // 8)
+                ],
+                axis=0,
+            )
+            snd_o[layer, q] = part.reshape(2, half, tile).astype(BF16)
             send_sums(layer, q)
         mark("update2")
         lax.fori_loop(lheads // 2, lheads * 3 // 4, update, 0)
         mark("wait_o")
-        for q in range(tiles):
-            if layer:
-                total = stream[layer - 1, q, tp].astype(F32)
-            else:
-                total = tokens_ref[tp, :, q * tile : (q + 1) * tile].astype(F32)
-            total = total + snd_o[layer, q, tp].astype(F32)
-            wait_sums(layer, q)
-            for k in range(nt - 1):
-                total = total + rcv_o[layer, q, k].astype(F32)
-            stream[layer, q, tp] = total.astype(BF16)
-            send_rows(layer, q)
+
+        @pl.when(owner)
+        def add_up(layer=layer):
+            for q in range(tiles):
+                if layer:
+                    total = stream[layer - 1, q, own].astype(F32)
+                else:
+                    total = tokens_ref[own, :, q * tile : (q + 1) * tile].astype(F32)
+                total = total + snd_o[layer, q, own].astype(F32)
+                wait_sums(layer, q)
+                for k in range(nt - 1):
+                    total = total + rcv_o[layer, q, k].astype(F32)
+                stream[layer, q, own] = total.astype(BF16)
+                send_rows(layer, q)
+
         if layer + 1 == layers:
             mark("update3")
             lax.fori_loop(lheads * 3 // 4, lheads, update, 0)
@@ -466,12 +528,10 @@
         wait_rows(layers - 1, q)
         out_ref[:, :, q * tile : (q + 1) * tile] = stream[layers - 1, q]
     mark("final")
-    for copy in pending:
-        copy.wait_send()
-    for layer in range(layers):
-        for ref, sems in ((snd_o, (rss, rsr)), (stream, (tgs, tgr))):
-            held = ref.at[layer, :, 0 : nt - 1]
-            tp_copy(held, held, sems, layer, 0, 0).wait_send()
+    for key in list(flying):
+        settle(key, [])
+    sent_sums(layers - 1)
+    sent_rows(layers - 1)
     mark(None)
 
 
@@ -503,7 +563,7 @@
     layers = w_z.shape[0]
     batch, dloc = tokens.shape
     seqs = lengths.shape[0]
-    rows = batch // nt
+    half = batch // 2
     width = w_x.shape[2]
     keys = w_b.shape[2]
     turned = jnp.swapaxes(w_dt, 1, 2)
@@ -524,14 +584,14 @@
     stream, kept, new = pl.pallas_call(
         functools.partial(block_kernel, nd, nt),
         out_shape=(
-            pltpu.VMEM((nt, rows, dloc), BF16),
+            pltpu.VMEM((2, half, dloc), BF16),
             pltpu.VMEM((layers, CONV_W - 1, seqs, conv_w), BF16),
             pltpu.VMEM(ssm_state.shape, F32),
         ),
         in_specs=[hbm] * 16,
         out_specs=[vmem] * 3,
         scratch_shapes=[
-            pltpu.VMEM((nt, rows, dloc), BF16),
+            pltpu.VMEM((2, half, dloc), BF16),
             pltpu.VMEM((1, seqs), jnp.int32),
             pltpu.VMEM(norm_gain.shape, F32),
             pltpu.VMEM(dt_bias.shape, F32),
@@ -551,33 +611,31 @@
             *parts(nx)[2:],
             *parts(max(nx - 1, 1))[2:],
             *parts(max(nx - 1, 1))[2:],
-            pltpu.VMEM((layers, nd, seqs, width), BF16),
-            *[pltpu.VMEM((layers, tiles, n, rows, tile), BF16) for n in (nt, nt - 1, nt)],
+            pltpu.VMEM((layers, seqs // 8, nd, 8, width), BF16),
+            *[pltpu.VMEM((layers, tiles, n, half, tile), BF16) for n in (2, nt - 1, 2)],
             *[pltpu.VMEM((batch, n), F32) for n in (heads_all, keys, width, keys, width)],
             pltpu.VMEM((seqs, conv_w), F32),
-            pltpu.VMEM((seqs, keys), F32),
-            pltpu.VMEM((seqs, width), F32),
             pltpu.VMEM((width // WIDTH_X, seqs, STATE), F32),
             pltpu.VMEM((width, 128), F32),
-            dma((layers, 6)),
+            dma((5 + layers,)),
             dma((layers,)),
             dma((9,)),
-            dma((layers, 3)),
-            dma((layers, 3)),
-            dma((layers, 3, max(nx - 1, 1))),
-            dma((layers, 3, max(nx - 1, 1))),
-            dma((layers, 3)),
-            dma((layers, 3)),
-            dma((layers,)),
-            dma((layers, tiles)),
-            dma((layers,)),
-            dma((layers, tiles)),
+            dma((3,)),
+            dma((3,)),
+            dma((3, max(nx - 1, 1))),
+            dma((3, max(nx - 1, 1))),
+            dma((2 + seqs // 8,)),
+            dma((2 + seqs // 8,)),
+            dma((2,)),
+            dma((tiles,)),
+            dma((1,)),
+            dma((tiles, 2)),
         ],
         compiler_params=pltpu.CompilerParams(
             collective_id=0, has_side_effects=True, vmem_limit_bytes=40 * 1024 * 1024
         ),
     )(
-        tokens.reshape(nt, rows, dloc), lengths[None, :], norm_gain, dt_bias, a_log, d_skip,
+        tokens.reshape(2, half, dloc), lengths[None, :], norm_gain, dt_bias, a_log, d_skip,
         out_gain, conv_weight, past, w_z, w_x, w_b, w_c, turned, w_out, ssm_state,
     )
     mixed_out, conv_new, ssm_new = pl.pallas_call(

time: 48 us -> 46.8 us (0.975)
  Pallas kernels: 47.2 us -> 46 us
    pallas_call x1, Pallas kernels: 41.3 us -> 40 us  [body(): pl.pallas_call(functools.partial(block_kernel, nd, nt), out_shape=(pltpu....]
where the time goes in v3:
time: 46.8 us; the launch traced here: 46.6 us
  Pallas kernels  46 us (98%)
  between operations  0.65 us (1%)
    pallas_call x1, Pallas kernels, body(): pl.pallas_call(functools.partial(block_kernel, nd, nt), out_shape=(pltpu....  40 us
    pallas_call x1, Pallas kernels, body(): pl.pallas_call(store_kernel, out_shape=(jax.ShapeDtypeStruct(stream.shape...  5.98 us

profile of v3, /device:TPU:0, one launch (start us, length us, event | category | flops | bytes accessed | tf_op | source)
XLA Modules:
  0.0 46.6 jit_solution(13757027253485750152)
XLA Ops:
  0.6 40.0 %shard_map.175 = (bf16[2,32,1024]{2,1,0:T(8,128)(2,1)S(1)}, bf16[2,3,16,2048]{3,2,1,0:T(8,128)(2,1)S(1)}, f32[2,16,16,64,128]{4,3,2,1,0:T(8,128)S(1)}) custom-call(bf16[2,32,1024]{2,1,0:T(8,128)(2,1)} %bitcast.8, s32[1,16]{1,0:T(1,128)} %bitcast.9, f32[2,1024]{1,0:T(2,128)} %gain_hbm.1, f32[2,16]{1,0:T(2,128)} %bias_hbm.1, f32[2,16]{1,0:T(2,128)} %alog_hbm.1, ...), custom_call_target="tpu_custom_call" | custom-call | tf_op jit(solution)/shard_map/pallas_call | solution.py:584
  40.7 6.0 %shard_map.176 = (bf16[2,32,1024]{2,1,0:T(8,128)(2,1)}, bf16[2,3,16,2048]{3,2,1,0:T(8,128)(2,1)}, f32[2,16,16,64,128]{4,3,2,1,0:T(8,128)}) custom-call(bf16[2,32,1024]{2,1,0:T(8,128)(2,1)S(1)} %get-tuple-element.9.stream_ref, bf16[2,3,16,2048]{3,2,1,0:T(8,128)(2,1)S(1)} %get-tuple-element.10.kept_ref, f32[2,16,16,64,128]{4,3,2,1,0:T(8,128)S(1)} %get-tuple-element.11.state_ref), custom_call_target="tpu_custom_call" | custom-call | tf_op jit(solution)/shard_map/pallas_call | solution.py:641
